TPU v7x, 32 devices: a whole 2x2x4 slice. The times are simulated.
32 devices in a mesh: ep: 4 (over y, x), tp: 8 (over z, core).
Axes of the slice: x: 2, y: 2, z: 4, core: 2. Of those that a mesh axis runs over, the one named last changes fastest.
Arguments:
- queries: bfloat16 [4096, 1024], P('ep', 'tp'), may hold values from -12 to 12
- keys: bfloat16 [4096, 1024], P('ep', 'tp'), may hold values from -12 to 12
- values: bfloat16 [4096, 2048], P('ep', 'tp'), may hold values from -6 to 6
- out_gate: bfloat16 [4096, 2048], P('ep', 'tp'), may hold values from -6 to 6
- in_gate: float32 [16, 4096], P('tp', 'ep'), may hold values from -8 to 100
- forget_gate: float32 [16, 4096], P('tp', 'ep'), may hold values from 0 to 16
- out_gain: float32 [2048], P('tp'), may hold values from 0.1 to 1.9
- out_weight: bfloat16 [2048, 4096], P('tp'), may hold values from -0.1875 to 0.1875
- moe_rows: bfloat16 [512, 4096], P('ep'), may hold values from -36 to 36
- moe_gain: float32 [4096], replicated, may hold values from 0.1 to 1.9
- routes: int32 [512, 2], P('ep'), may hold values from 0 to 3, all different within a row; in each aligned block of 128 rows (0 to 127, 128 to 255, ...) at most 96 rows name the same one
- route_weight: float32 [512, 2], P('ep'), may hold values from 0.2 to 1.2
- expert_gate: bfloat16 [4, 4096, 4096], P('ep', None, 'tp'), may hold values from -0.09375 to 0.09375
- expert_up: bfloat16 [4, 4096, 4096], P('ep', None, 'tp'), may hold values from -0.09375 to 0.09375
- expert_down: bfloat16 [4, 4096, 4096], P('ep', 'tp'), may hold values from -0.125 to 0.125
- shared_gate: bfloat16 [4096, 2048], P(None, 'tp'), may hold values from -0.09375 to 0.09375
- shared_up: bfloat16 [4096, 2048], P(None, 'tp'), may hold values from -0.09375 to 0.09375
- shared_down: bfloat16 [2048, 4096], P('tp'), may hold values from -0.1875 to 0.1875
Outputs:
- mixer_out: bfloat16 [4096, 4096], P('ep', 'tp')
- moe_out: bfloat16 [512, 4096], P('ep', 'tp')
Inputs may be any that keep to these rules, and one draw needn't show every extreme that they name: `routes`: each row names 2 different experts. Within the 128 rows of one index of ep no expert is named more than 96 times, a bound that some block reaches.
All inputs are finite; a program needn't handle non-finite values.
Results may differ from a plain program's by a relative error of at most 0.019.
Values may be sent and summed in bfloat16 or wider, within the bound.
A program may use at most 128 MiB of HBM per device.

v0:
```python
import jax
import jax.numpy as jnp
from jax import lax
from jax.sharding import PartitionSpec as P

DK = 64
DV = 128
BLK = 64


highest = lax.Precision.HIGHEST
far_below = -1e30


def carried_in(value, axis, combine, identity):
    length, position = (lax.axis_size(axis), lax.axis_index(axis))
    everything = jax.tree.map(lambda part: lax.all_gather(part, axis), value)
    start = jax.tree.map(
        lambda part, zero: jnp.broadcast_to(jnp.asarray(zero, part.dtype), part.shape),
        value,
        identity,
    )

    def lap(k, before):
        reached = k < position
        new = combine(before, jax.tree.map(lambda part: part[k], everything))
        return jax.tree.map(lambda a, b: jnp.where(reached, a, b), new, before)

    return lax.fori_loop(0, length, lap, start)


def combine_state(earlier, later_part):
    decay_a, matrix_a, normal_a, stab_a = earlier
    decay_b, matrix_b, normal_b, stab_b = later_part
    joined = jnp.maximum(decay_b + stab_a, stab_b)
    weight_a = jnp.exp(decay_b + stab_a - joined)
    weight_b = jnp.exp(stab_b - joined)
    return (
        decay_a + decay_b,
        weight_a[..., None, None] * matrix_a + weight_b[..., None, None] * matrix_b,
        weight_a[..., None] * normal_a + weight_b[..., None] * normal_b,
        joined,
    )


def memory_cells(queries, keys, values, in_gate, forget_gate):
    tok_rows = queries.shape[0]
    head_count = in_gate.shape[0]
    block_count = tok_rows // BLK
    scale = DK ** (-0.5)
    query_block = queries.reshape(block_count, BLK, head_count, DK)
    key_block = keys.reshape(block_count, BLK, head_count, DK)
    value_block = values.reshape(block_count, BLK, head_count, DV)
    gate_in = in_gate.reshape(head_count, block_count, BLK).transpose(1, 0, 2)
    log_forget = (
        jax.nn.log_sigmoid(forget_gate).reshape(head_count, block_count, BLK).transpose(1, 0, 2)
    )
    cumulative = jnp.cumsum(log_forget, axis=2)
    block_last = cumulative[:, :, -1]
    state_logs = block_last[..., None] - cumulative + gate_in
    block_top = jnp.max(state_logs, axis=2)
    state_weight = jnp.exp(state_logs - block_top[..., None])
    key_wide = key_block.astype(jnp.float32)
    weighted = state_weight.transpose(0, 2, 1)[..., None] * value_block.astype(jnp.float32)
    block_matrix = jnp.einsum("nlhv,nlhk->nhvk", weighted, key_wide, precision=highest)
    block_normal = jnp.einsum("nhl,nlhk->nhk", state_weight, key_wide, precision=highest)
    identity_state = (
        jnp.zeros((head_count,), jnp.float32),
        jnp.zeros((head_count, DV, DK), jnp.float32),
        jnp.zeros((head_count, DK), jnp.float32),
        jnp.full((head_count,), far_below, jnp.float32),
    )

    def fold_block(running, summary):
        return (combine_state(running, summary), running)

    device_total, before = lax.scan(
        fold_block, identity_state, (block_last, block_matrix, block_normal, block_top)
    )
    prefix = carried_in(device_total, "ep", combine_state, identity_state)
    anchor = (
        identity_state[0],
        identity_state[1],
        identity_state[2],
        jnp.zeros((head_count,), jnp.float32),
    )
    entering = combine_state(combine_state(anchor, prefix), before)
    matrix_in = entering[1]
    normal_in = entering[2]
    stab_in = entering[3]
    causal = jnp.tril(jnp.ones((BLK, BLK), dtype=bool))
    intra_logs = cumulative[..., :, None] - cumulative[..., None, :] + gate_in[..., None, :]
    intra_logs = jnp.where(causal, intra_logs, -jnp.inf)
    inter_logs = cumulative + stab_in[..., None]
    stabilizer = jnp.maximum(inter_logs, jnp.max(intra_logs, axis=3))
    raw_scores = jnp.einsum(
        "nthd,nshd->nhts", query_block, key_block, preferred_element_type=jnp.float32
    )
    scores = raw_scores * scale * jnp.exp(intra_logs - stabilizer[..., None])
    inner = jnp.einsum(
        "nhts,nshv->nthv",
        scores.astype(jnp.bfloat16),
        value_block,
        preferred_element_type=jnp.float32,
    )
    query_wide = query_block.astype(jnp.float32) * scale
    across = jnp.einsum("nthk,nhvk->nthv", query_wide, matrix_in, precision=highest)
    inter_weight = jnp.exp(inter_logs - stabilizer)
    normal_dot = jnp.einsum("nthk,nhk->nht", query_wide, normal_in, precision=highest)
    signed = jnp.sum(scores, axis=3) + inter_weight * normal_dot
    divisor = jnp.maximum(jnp.abs(signed), jnp.exp(-stabilizer)).transpose(0, 2, 1)
    numer = inner + inter_weight.transpose(0, 2, 1)[..., None] * across
    return (numer / divisor[..., None]).reshape(tok_rows, head_count * DV)


def local(
    queries,
    keys,
    values,
    out_gate,
    in_gate,
    forget_gate,
    out_gain,
    out_weight,
    moe_rows,
    moe_gain,
    routes,
    route_weight,
    expert_gate,
    expert_up,
    expert_down,
    shared_gate,
    shared_up,
    shared_down,
):
    tok_rows = queries.shape[0]
    tp_count = lax.axis_size("tp")
    ep_count = lax.axis_size("ep")
    col_width = out_weight.shape[1] // tp_count
    cells = memory_cells(queries, keys, values, in_gate, forget_gate)
    mixed = (cells * jax.nn.sigmoid(out_gate.astype(jnp.float32)) * out_gain).astype(jnp.bfloat16)
    blocks_here = tok_rows * lax.axis_size("tp") // tok_rows
    product = jnp.dot(mixed, out_weight, preferred_element_type=jnp.float32)
    mixer_out = lax.psum_scatter(
        product.reshape(tok_rows, blocks_here, col_width)
        .transpose(1, 0, 2)
        .reshape(tok_rows * lax.axis_size("tp"), col_width)
        .astype(jnp.bfloat16),
        "tp",
        scatter_dimension=0,
        tiled=True,
    )
    routed_rows = moe_rows.shape[0]
    topk_count = routes.shape[1]
    local_experts = expert_gate.shape[0]
    expert_count = local_experts * ep_count
    capacity = 3 * routed_rows * topk_count // (2 * expert_count)
    rows_wide = moe_rows.astype(jnp.float32)
    inverse = lax.rsqrt(jnp.mean(rows_wide * rows_wide, axis=1, keepdims=True) + 1e-06)
    normed = (rows_wide * inverse * moe_gain).astype(jnp.bfloat16)
    flat_routes = routes.reshape(-1)
    onehot = (flat_routes[:, None] == jnp.arange(expert_count, dtype=jnp.int32)[None, :]).astype(
        jnp.int32
    )
    token_position = jnp.sum(jnp.cumsum(onehot, axis=0) * onehot, axis=1) - 1
    destination = flat_routes * capacity + token_position
    token_of = jnp.arange(flat_routes.shape[0], dtype=jnp.int32) // topk_count
    slot_row = jnp.zeros((expert_count * capacity,), jnp.int32).at[destination].set(token_of)
    outgoing = normed[slot_row].reshape(ep_count, local_experts * capacity, normed.shape[1])
    arrived = lax.all_to_all(outgoing, "ep", split_axis=0, concat_axis=0, tiled=True)
    arrived = arrived.reshape(ep_count, local_experts, capacity, normed.shape[1])
    gate_val = jnp.einsum(
        "sjcd,jdf->jscf", arrived, expert_gate, preferred_element_type=jnp.float32
    )
    up_val = jnp.einsum("sjcd,jdf->jscf", arrived, expert_up, preferred_element_type=jnp.float32)
    hidden = (jax.nn.silu(gate_val) * up_val).astype(jnp.bfloat16)
    shared_gate_val = jnp.dot(normed, shared_gate, preferred_element_type=jnp.float32)
    shared_up_val = jnp.dot(normed, shared_up, preferred_element_type=jnp.float32)
    shared_hidden = (jax.nn.silu(shared_gate_val) * shared_up_val).astype(jnp.bfloat16)
    slot_count = ep_count * local_experts * capacity
    total_rows = slot_count + routed_rows
    feat_width = moe_rows.shape[1] // tp_count
    blocks_here = total_rows * lax.axis_size("tp") // total_rows
    routed_part = jnp.einsum(
        "jscf,jfo->sjco", hidden, expert_down, preferred_element_type=jnp.float32
    )
    routed_part = routed_part.reshape(slot_count, blocks_here * feat_width)
    shared_part = jnp.dot(shared_hidden, shared_down, preferred_element_type=jnp.float32)
    joined_rows = jnp.concatenate([routed_part, shared_part], axis=0)
    summed = lax.psum_scatter(
        joined_rows.reshape(total_rows, blocks_here, feat_width)
        .transpose(1, 0, 2)
        .reshape(total_rows * lax.axis_size("tp"), feat_width)
        .astype(jnp.bfloat16),
        "tp",
        scatter_dimension=0,
        tiled=True,
    ).astype(jnp.float32)
    routed_total = summed[:slot_count]
    shared_total = summed[slot_count:]
    routed_sum = routed_total.astype(jnp.bfloat16).reshape(
        ep_count, local_experts * capacity, feat_width
    )
    returned = lax.all_to_all(routed_sum, "ep", split_axis=0, concat_axis=0, tiled=True)
    returned = returned.reshape(expert_count * capacity, feat_width)
    picked = returned[destination].astype(jnp.float32).reshape(routed_rows, topk_count, feat_width)
    moe_out = (jnp.sum(picked * route_weight[:, :, None], axis=1) + shared_total).astype(
        jnp.bfloat16
    )
    return (mixer_out, moe_out)


def solution(mesh):
    return jax.shard_map(
        local,
        mesh=mesh,
        in_specs=(
            P("ep", "tp"),
            P("ep", "tp"),
            P("ep", "tp"),
            P("ep", "tp"),
            P("tp", "ep"),
            P("tp", "ep"),
            P("tp"),
            P("tp", None),
            P("ep", None),
            P(),
            P("ep", None),
            P("ep", None),
            P("ep", None, "tp"),
            P("ep", None, "tp"),
            P("ep", "tp", None),
            P(None, "tp"),
            P(None, "tp"),
            P("tp", None),
        ),
        out_specs=(P("ep", "tp"), P("ep", "tp")),
        check_vma=False,
    )
```

profile of v0, /device:TPU:0, one launch (start us, length us, event | category | flops | bytes accessed | tf_op | source)
XLA Modules:
  0.0 280.3 jit_solution(3931969041635986831)
XLA Ops:
  9.1 1.2 reduce-window.6
  11.0 1.4 scatter_custom_fusion
  12.4 1.5 fusion.23
  14.0 1.6 fusion.25
  15.5 4.1 %gather_fusion = bf16[384,4096]{1,0:T(8,128)(2,1)} fusion(bf16[128,4096]{1,0:T(8,128)(2,1)S(1)} %fusion.25, s32[1024]{0:T(1024)S(1)} %pad_clamp_fusion.1), kind=kCustom, calls=%fused_computation | custom fusion | bytes 6292992 | tf_op jit(solution)/shard_map/gather | solution.py:169
  19.6 5.3 %all-to-all-start = ((bf16[4,96,4096]{2,1,0:T(8,128)(2,1)}), bf16[4,96,4096]{2,1,0:T(8,128)(2,1)}, u32[]{:S(2)}, u32[]{:S(2)}) async-start(bf16[4,96,4096]{2,1,0:T(8,128)(2,1)} %bitcast.227), calls=%async_computation.1 | async-start | bytes 6291456 | tf_op jit(solution)/shard_map/all_to_all | solution.py:170
  26.4 2.0 reshape.171
  28.4 2.0 reshape.174
  30.4 2.0 fusion.102
  32.5 4.5 %convolution_convert_fusion.2 = bf16[128,4096]{1,0:T(8,128)(2,1)} fusion(bf16[256,4096]{1,0:T(8,128)(2,1)} %param.39, bf16[128,4096]{1,0:T(8,128)(2,1)S(1)} %fusion.25, bf16[4096,256]{1,0:T(8,128)(2,1)} %param.38, f32[128,256]{1,0:T(8,128)S(1)} %fusion.102), kind=kOutput, calls=%fused_computation.45 | convolution fusion | flops 537591808 | bytes 6422528 | tf_op jit(solution)/shard_map/dot_general | solution.py:188
  37.0 1.7 copy.119
  39.3 3.5 %fusion.52 = f32[16,2,128,64]{3,2,1,0:T(8,128)} fusion(f32[16,64,2]{1,2,0:T(2,128)S(1)} %copy.79, bf16[16,64,2,128]{3,2,1,0:T(2,128)(2,1)S(1)} %copy-done.2, bf16[16,64,2,64]{3,2,1,0:T(2,128)(2,1)S(1)} %copy-done.4), kind=kOutput, calls=%fused_computation.80 | convolution fusion | flops 201850880 | bytes 1843200 | tf_op jit(solution)/shard_map/nlhv,nlhk->nhvk/dot_general | solution.py:65
  42.8 19.3 %all-to-all-done = bf16[4,96,4096]{2,1,0:T(8,128)(2,1)} async-done(((bf16[4,96,4096]{2,1,0:T(8,128)(2,1)}), bf16[4,96,4096]{2,1,0:T(8,128)(2,1)}, u32[]{:S(2)}, u32[]{:S(2)}) %all-to-all-start) | async-done | bytes 3145760 | tf_op jit(solution)/shard_map/all_to_all | solution.py:170
  62.1 5.8 %fusion.21 = f32[4,96,512]{2,1,0:T(8,128)} fusion(bf16[4,96,4096]{2,1,0:T(8,128)(2,1)} %all-to-all-done, bf16[1,4096,512]{2,1,0:T(8,128)(2,1)} %param.34), kind=kOutput, calls=%fused_computation.50 | convolution fusion | flops 1610612736 | bytes 8126464 | tf_op jit(solution)/shard_map/sjcd,jdf->jscf/dot_general | solution.py:172
  67.9 9.8 %convolution_convert_fusion.1 = bf16[4,96,4096]{2,1,0:T(8,128)(2,1)} fusion(bf16[1,512,4096]{2,1,0:T(8,128)(2,1)} %param.36, bf16[4,96,4096]{2,1,0:T(8,128)(2,1)} %all-to-all-done, bf16[1,4096,512]{2,1,0:T(8,128)(2,1)} %param.35, f32[4,96,512]{2,1,0:T(8,128)} %fusion.21), kind=kOutput, calls=%fused_computation.44 | convolution fusion | flops 3223977984 | bytes 15466496 | tf_op jit(solution)/shard_map/jscf,jfo->sjco/dot_general | solution.py:184
  77.7 3.3 %copy.118 = bf16[48,8,8,512]{3,2,1,0:T(8,128)(2,1)S(1)} copy(bf16[48,8,8,512]{3,1,2,0:T(8,128)(2,1)} %bitcast.232) | data formatting | bytes 6291456
  81.4 3.4 %copy.105 = bf16[8,512,512]{2,1,0:T(8,128)(2,1)} copy(bf16[8,512,512]{2,0,1:T(8,128)(2,1)S(1)} %maximum_bitcast_fusion) | data formatting | bytes 8388608 | tf_op jit(solution)/shard_map/convert_element_type | solution.py:194
  85.1 30.0 %while.45 = (s32[]{:T(128)}, f32[2]{0:T(128)S(1)}, f32[2,128,64]{2,1,0:T(8,128)S(1)}, f32[2,64]{1,0:T(2,128)S(1)}, f32[2]{0:T(128)S(1)}, /*index=5*/f32[16,2]{1,...) while((s32[]{:T(128)}, f32[2]{0:T(128)S(1)}, ...), condition=%wide.region_3.4_spmd.clone, body=%wide.region_2.3_spmd.clone.sunk | while | flops 82577 | bytes 397655 | solution.py:77
  85.8 1.0 fusion.117
  87.6 1.0 fusion.117
  89.5 1.0 fusion.117
  91.4 1.0 fusion.117
  93.3 1.0 fusion.117
  95.1 1.0 fusion.117
  97.0 1.0 fusion.117
  98.9 1.0 fusion.117
  100.8 1.0 fusion.117
  102.6 1.0 fusion.117
  104.5 1.0 fusion.117
  108.3 1.0 fusion.117
  110.1 1.0 fusion.117
  113.9 1.0 fusion.117
  116.8 9.0 %all-reduce.2 = (f32[8]{0:T(128)S(1)}, f32[8]{0:T(128)S(1)}) all-reduce(f32[8]{0:T(128)S(1)} %dynamic-update-slice, f32[8]{0:T(128)S(1)} %dynamic-update-slice.1), channel_id=2, replica_groups=mesh['ep'=4,'tp'=8] {'ep'}, use_global_device_ids=true, to_apply=%add | all-reduce | flops 16 | bytes 128
  126.0 8.0 %all-gather.4 = f32[4,2,64]{2,1,0:T(2,128)S(1)} all-gather(f32[1,2,64]{2,1,0:T(2,128)S(1)} %bitcast.236), channel_id=5, replica_groups=mesh['ep'=4,'tp'=8] {'ep'}, dimensions={0}, use_global_device_ids=true | all-gather | bytes 2560 | tf_op jit(solution)/shard_map/all_gather | solution.py:17
  134.0 8.0 %all-gather.2 = f32[8,128,64]{1,2,0:T(8,128)S(1)} all-gather(f32[2,128,64]{1,2,0:T(8,128)S(1)} %copy.85), channel_id=4, replica_groups=mesh['ep'=4,'tp'=8] {'ep'}, dimensions={0}, use_global_device_ids=true | all-gather | bytes 327680 | tf_op jit(solution)/shard_map/all_gather | solution.py:17
  142.1 1.4 while.46
  144.4 1.2 reshape.170
  145.8 1.8 fusion.48
  149.1 4.4 %fusion.36 = f32[16,64,2,128]{3,1,2,0:T(8,128)S(1)} fusion(f32[16,2,128,64]{3,2,1,0:T(8,128)S(1)} %copy-done.1, f32[16,2]{1,0:T(8,128)S(1)} %subtract_exponential_fusion.4, f32[2,128,64]{2,1,0:T(8,128)S(1)} %multiply_add_fusion, f32[16,2]{1,0:T(8,128)S(1)} %get-tuple-element.436, f32[16,64,2]{1,2,0:T(2,128)S(1)} %copy.93, ...), kind=kOutput, calls=%fused_computation.67 | convolution fusion | flops 202637312 | bytes 2433280 | tf_op jit(solution)/shard_map/nthk,nhvk->nthv/dot_general | solution.py:107
  155.6 5.6 %convolution_convert_fusion = bf16[1024,4096]{1,0:T(8,128)(2,1)} fusion(bf16[256,4096]{1,0:T(8,128)(2,1)S(1)} %copy-done, f32[128,8,2,128]{3,2,1,0:T(2,128)S(1)} %bitcast.234, bf16[1024,256]{1,0:T(8,128)(2,1)S(1)} %copy-done.9, f32[256]{0:T(256)S(1)} %copy-done.10), kind=kOutput, calls=%fused_computation.43 | convolution fusion | flops 2153512960 | bytes 12059648 | tf_op jit(solution)/shard_map/dot_general | solution.py:143
  161.2 12.2 %copy.116 = bf16[128,8,8,512]{3,2,1,0:T(8,128)(2,1)} copy(bf16[128,8,8,512]{3,1,2,0:T(8,128)(2,1)} %bitcast.229) | data formatting | bytes 16777216
  173.3 9.5 %copy.99 = bf16[8,1024,512]{2,1,0:T(8,128)(2,1)} copy(bf16[8,1024,512]{2,0,1:T(8,128)(2,1)} %bitcast.224) | data formatting | bytes 16777216 | tf_op jit(solution)/shard_map/convert_element_type | solution.py:148
  182.9 1.8 slice.31
  184.7 3.5 %all-to-all-start.1 = ((bf16[4,96,512]{2,1,0:T(8,128)(2,1)}), bf16[4,96,512]{2,1,0:T(8,128)(2,1)S(1)}, u32[]{:S(2)}, u32[]{:S(2)}) async-start(bf16[4,96,512]{2,1,0:T(8,128)(2,1)} %bitcast.37), calls=%async_computation.3 | async-start | bytes 786432 | tf_op jit(solution)/shard_map/all_to_all | solution.py:204
  188.3 5.7 %all-to-all-done.1 = bf16[4,96,512]{2,1,0:T(8,128)(2,1)S(1)} async-done(((bf16[4,96,512]{2,1,0:T(8,128)(2,1)}), bf16[4,96,512]{2,1,0:T(8,128)(2,1)S(1)}, u32[]{:S(2)}, u32[]{:S(2)}) %all-to-all-start.1) | async-done | bytes 393248 | tf_op jit(solution)/shard_map/all_to_all | solution.py:204
  194.0 1.2 gather_fusion.1
  196.2 1.6 add_convert_fusion
  197.8 75.2 %reduce-scatter.3.cloned.1.call-done = bf16[1024,512]{1,0:T(8,128)(2,1)} async-done(((bf16[8192,512]{1,0:T(8,128)(2,1)}), bf16[1024,512]{1,0:T(8,128)(2,1)}) %reduce-scatter.3.cloned.1.call-update) | async-done | bytes 1048592 | tf_op jit(solution)/shard_map/reduce_scatter | solution.py:144
  (244 shorter events, 29.5 us)
Async XLA Ops:
  7.2 148.2 %copy-start = (bf16[256,4096]{1,0:T(8,128)(2,1)S(1)}, bf16[256,4096]{1,0:T(8,128)(2,1)}, u32[]{:S(2)}) copy-start(bf16[256,4096]{1,0:T(8,128)(2,1)} %param.29) | copy-start | bytes 6291460
  19.6 5.6 %copy-start.7 = (f32[2,1024]{1,0:T(2,128)S(1)}, f32[2,1024]{1,0:T(2,128)}, u32[]{:S(2)}) copy-start(f32[2,1024]{1,0:T(2,128)} %param.27) | copy-start | bytes 24580
  19.6 5.7 %copy-start.6 = (f32[2,1024]{1,0:T(2,128)S(1)}, f32[2,1024]{1,0:T(2,128)}, u32[]{:S(2)}) copy-start(f32[2,1024]{1,0:T(2,128)} %param.26) | copy-start | bytes 24580
  19.6 42.5 %all-to-all-start = ((bf16[4,96,4096]{2,1,0:T(8,128)(2,1)}), bf16[4,96,4096]{2,1,0:T(8,128)(2,1)}, u32[]{:S(2)}, u32[]{:S(2)}) async-start(bf16[4,96,4096]{2,1,0:T(8,128)(2,1)} %bitcast.227), calls=%async_computation.1 | async-start | bytes 6291456 | tf_op jit(solution)/shard_map/all_to_all | solution.py:170
  24.9 158.0 %reduce-scatter.5.cloned.1.call-start = ((), (), s32[]{:S(2)}) async-start(), calls=%async_computation.5 | async-start | bytes 4718592 | tf_op jit(solution)/shard_map/reduce_scatter | solution.py:190
  37.0 1.8 copy-start.4
  37.0 2.3 copy-start.2
  84.8 30.3 %copy-start.11 = (u32[32]{0:T(128)S(1)}, u32[32]{0:T(128)}, u32[]{:S(2)}) copy-start(u32[32]{0:T(128)} %constant.119) | copy-start | bytes 388
  84.8 188.2 %reduce-scatter.3.cloned.1.call-start = ((), (), s32[]{:S(2)}) async-start(), calls=%async_computation.4 | async-start | bytes 9437184 | tf_op jit(solution)/shard_map/reduce_scatter | solution.py:144
  142.1 5.5 %copy-start.5 = (bf16[16,64,2,64]{3,2,1,0:T(2,128)(2,1)S(1)}, bf16[16,64,2,64]{3,2,1,0:T(2,128)(2,1)}, u32[]{:S(2)}) copy-start(bf16[16,64,2,64]{3,2,1,0:T(2,128)(2,1)} %reshape.171) | copy-start | bytes 786436
  147.5 1.6 copy-start.1
  148.4 5.1 %copy-start.3 = (bf16[16,64,2,128]{3,2,1,0:T(2,128)(2,1)S(1)}, bf16[16,64,2,128]{3,2,1,0:T(2,128)(2,1)}, u32[]{:S(2)}) copy-start(bf16[16,64,2,128]{3,2,1,0:T(2,128)(2,1)} %reshape.174) | copy-start | bytes 1572868
  154.5 1.0 copy-start.9
  154.5 1.0 copy-start.10
  182.9 5.3 %copy-start.8 = (f32[128,2]{0,1:T(2,128)S(1)}, f32[128,2]{0,1:T(2,128)}, u32[]{:S(2)}) copy-start(f32[128,2]{0,1:T(2,128)} %param.33) | copy-start | bytes 3076
  184.7 9.3 %all-to-all-start.1 = ((bf16[4,96,512]{2,1,0:T(8,128)(2,1)}), bf16[4,96,512]{2,1,0:T(8,128)(2,1)S(1)}, u32[]{:S(2)}, u32[]{:S(2)}) async-start(bf16[4,96,512]{2,1,0:T(8,128)(2,1)} %bitcast.37), calls=%async_computation.3 | async-start | bytes 786432 | tf_op jit(solution)/shard_map/all_to_all | solution.py:204
Sparse Core Ops, SparseCore 0:
  84.9 50.3 reduce-scatter.4
  183.0 89.9 reduce-scatter.2
where the time goes:
time: 285 us; the launch traced here: 280 us
  waiting for transfers between devices  100 us (35%)
  local copies, waits for them, and re-layouts  51.1 us (18%)
  matrix products  39.7 us (14%)
  other arithmetic  39.1 us (14%)
  blocking collectives  25 us (9%)
  between operations  15.6 us (5%)
  starting transfers between devices  9.2 us (3%)
    reduce_scatter x1, waiting for transfers between devices, local(): lax.psum_scatter(product.reshape(tok_rows, blocks_here, col_width).transp...  75.2 us
    unnamed x36, local copies, waits for them, and re-layouts  20.2 us
    all_to_all x1, waiting for transfers between devices, local(): lax.all_to_all(outgoing, 'ep', split_axis=0, concat_axis=0, tiled=True)  19.3 us
    all_gather x2, blocking collectives, carried_in(): everything = jax.tree.map(lambda part: lax.all_gather(part, axis), value)  16.1 us
    add x17, other arithmetic, combine_state(): weight_a[..., None, None] * matrix_a + weight_b[..., None, None] * matrix_b  15.9 us
    dynamic_update_slice x32, other arithmetic, memory_cells(): lax.scan(fold_block, identity_state, (block_last, block_matrix, block_nor...  10.8 us
    dot_general x1, matrix products, local(): jnp.einsum('jscf,jfo->sjco', hidden, expert_down, preferred_element_type=...  9.82 us
    convert_element_type x1, local copies, waits for them, and re-layouts, local(): mixer_out = lax.psum_scatter(product.reshape(tok_rows, blocks_here, col_w...  9.51 us
  transfers between devices with their start and end apart: 4, of which 3 were waited for; matrix products, arithmetic and copies ran while one was open for 34% of the time, Pallas kernels for 0%

commit v1 on v0

v1 whole, which is shorter than its diff:
```python
import functools

import jax
import jax.numpy as jnp
from jax import lax
from jax.experimental import pallas as pl
from jax.experimental.pallas import tpu as pltpu
from jax.sharding import PartitionSpec as P

DK = 64
DV = 128
CH = 128
F32 = jnp.float32
BF16 = jnp.bfloat16
VM = pl.BlockSpec(memory_space=pltpu.VMEM)


def gate_rows(ig, fg):
    lane = lax.broadcasted_iota(jnp.int32, ig.shape, 1)
    total = jnp.minimum(fg, 0.0) - jnp.log1p(jnp.exp(-jnp.abs(fg)))
    step = 1
    while step < CH:
        total = total + jnp.where(lane >= step, pltpu.roll(total, step, 1), 0.0)
        step *= 2
    level = ig - total
    top = level
    step = 1
    while step < CH:
        top = jnp.maximum(top, jnp.where(lane >= step, pltpu.roll(top, step, 1), -1e30))
        step *= 2
    return total, level, top


def columns_of(parts):
    rows = sum(part.shape[0] for part in parts)
    padded = -(-rows // 128) * 128
    if padded > rows:
        parts = list(parts) + [jnp.zeros((padded - rows, CH), F32)]
    return jnp.concatenate(parts, axis=0).T


def split_bf16(x):
    high = x.astype(BF16)
    return high, (x - high.astype(F32)).astype(BF16)


def weighted_keys(keys, cols, first, heads, chunks):
    lane_head = lax.broadcasted_iota(jnp.int32, keys.shape, 1) // DK
    weight = jnp.broadcast_to(cols[:, first : first + 1], keys.shape)
    for h in range(1, heads):
        at = first + h * chunks
        weight = jnp.where(lane_head == h, jnp.broadcast_to(cols[:, at : at + 1], keys.shape), weight)
    return split_bf16(keys.astype(F32) * weight)


def add_outer(kw, values):
    dims = (((0,), (0,)), ((), ()))
    return lax.dot_general(kw[0], values, dims, preferred_element_type=F32) + lax.dot_general(
        kw[1], values, dims, preferred_element_type=F32
    )


def pick_head(parts, shape, axis):
    head = lax.broadcasted_iota(jnp.int32, shape, axis) // DK
    out = jnp.broadcast_to(parts[0], shape)
    for h in range(1, len(parts)):
        out = jnp.where(head == h, jnp.broadcast_to(parts[h], shape), out)
    return out


def summary_kernel(heads, chunks, k_ref, v_ref, ig_ref, fg_ref, out_ref):
    width = heads * DK
    total, level, top = gate_rows(ig_ref[...], fg_ref[...])
    shape = total.shape
    chunk = lax.broadcasted_iota(jnp.int32, shape, 0) % chunks
    last = jnp.broadcast_to(total[:, CH - 1 : CH], shape)
    suffix = last
    step = 1
    while step < chunks:
        moved = pltpu.roll(suffix, shape[0] - step, 0)
        suffix = suffix + jnp.where(chunk + step < chunks, moved, 0.0)
        step *= 2
    reach = suffix + jnp.broadcast_to(top[:, CH - 1 : CH], shape)
    tops = [
        jnp.max(reach[h * chunks : (h + 1) * chunks], axis=0, keepdims=True) for h in range(heads)
    ]
    weight = [
        jnp.exp(
            level[h * chunks : (h + 1) * chunks] + suffix[h * chunks : (h + 1) * chunks] - tops[h]
        )
        for h in range(heads)
    ]
    cols = columns_of(weight)
    state = jnp.zeros((width, heads * DV + 128), F32)
    for c in range(chunks):
        rows = pl.ds(c * CH, CH)
        kw = weighted_keys(k_ref[rows, :], cols, c, heads, chunks)
        values = jnp.concatenate([v_ref[rows, :], jnp.ones((CH, 128), BF16)], axis=1)
        state = state + add_outer(kw, values)
    out_ref[...] = jnp.zeros_like(out_ref)
    out_ref[0:width, :] = pick_head(
        [state[:, h * DV : (h + 1) * DV] for h in range(heads)], (width, DV), 0
    )
    normal = state[:, heads * DV :].T
    out_ref[width : width + 1, 0:width] = normal[0:1, :]
    for h in range(heads):
        out_ref[width + 1 + h : width + 2 + h, :] = tops[h]
        at = width + 1 + heads + h
        out_ref[at : at + 1, :] = suffix[h * chunks : h * chunks + 1]


def cells_kernel(
    heads, chunks, pos_ref, q_ref, k_ref, v_ref, og_ref, ig_ref, fg_ref, gain_ref, sum_ref, out_ref
):
    width = heads * DK
    matrix = jnp.zeros((width, DV), F32)
    normal = jnp.zeros((1, width), F32)
    stab = [jnp.zeros((1, 128), F32) for _ in range(heads)]
    for e in range(sum_ref.shape[0]):
        reached = e < pos_ref[0]
        part = sum_ref.at[e]
        old_w, new_w, new_stab = [], [], []
        for h in range(heads):
            at = width + 1 + h
            carried = part[at + heads : at + heads + 1, :] + stab[h]
            there = part[at : at + 1, :]
            joined = jnp.maximum(carried, there)
            old_w.append(jnp.where(reached, jnp.exp(carried - joined), 1.0))
            new_w.append(jnp.where(reached, jnp.exp(there - joined), 0.0))
            new_stab.append(jnp.where(reached, joined, stab[h]))
        matrix = (
            pick_head(old_w, (width, DV), 0) * matrix
            + pick_head(new_w, (width, DV), 0) * part[0:width, :]
        )
        normal = (
            pick_head([w[:, 0:width] for w in old_w], (1, width), 1) * normal
            + pick_head([w[:, 0:width] for w in new_w], (1, width), 1)
            * part[width : width + 1, 0:width]
        )
        stab = new_stab
    normal_cols = jnp.broadcast_to(normal, (128, width)).T
    state = jnp.concatenate([matrix] * heads + [normal_cols], axis=1)

    total, level, top = gate_rows(ig_ref[...], fg_ref[...])
    shape = total.shape
    last = jnp.broadcast_to(total[:, CH - 1 : CH], shape)
    last_top = jnp.broadcast_to(top[:, CH - 1 : CH], shape)
    entering, leaving = [], []
    for h in range(heads):
        now = stab[h]
        for c in range(chunks):
            r = h * chunks + c
            entering.append(now)
            now = last[r : r + 1] + jnp.maximum(now, last_top[r : r + 1])
            leaving.append(now)
    entering = jnp.concatenate(entering, axis=0)
    leaving = jnp.concatenate(leaving, axis=0)
    peak = jnp.maximum(top, entering)
    decay = jnp.exp(last + entering - leaving)
    count = heads * chunks
    cols = columns_of(
        [
            peak,
            jnp.exp(entering - peak),
            jnp.exp(-(total + peak)),
            jnp.exp(last + level - leaving),
        ]
    )
    causal = lax.broadcasted_iota(jnp.int32, (CH, CH), 0) >= lax.broadcasted_iota(
        jnp.int32, (CH, CH), 1
    )
    lane_head = lax.broadcasted_iota(jnp.int32, (CH, width), 1) // DK
    for c in range(chunks):
        rows = pl.ds(c * CH, CH)
        keys = k_ref[rows, :]
        values = v_ref[rows, :]
        queries = q_ref[rows, :] * jnp.asarray(DK**-0.5, BF16)
        high, low = split_bf16(state)
        for h in range(heads):
            r = h * chunks + c
            mine = jnp.where(lane_head == h, queries, jnp.zeros_like(queries))
            raw = lax.dot_general(
                mine, keys, (((1,), (1,)), ((), ())), preferred_element_type=F32
            )
            logs = level[r : r + 1, :] - cols[:, r : r + 1]
            scores = raw * jnp.exp(jnp.where(causal, logs, -jnp.inf))
            inner = jnp.dot(
                scores.astype(BF16), values[:, h * DV : (h + 1) * DV], preferred_element_type=F32
            )
            across = 0.0
            for piece in (high, low):
                rhs = jnp.concatenate(
                    [piece[:, h * DV : (h + 1) * DV], piece[:, heads * DV :]], axis=1
                )
                across = across + jnp.dot(mine, rhs, preferred_element_type=F32)
            inter = cols[:, count + r : count + r + 1]
            signed = jnp.sum(scores, axis=1, keepdims=True) + inter * across[:, DV : DV + 1]
            divisor = jnp.maximum(jnp.abs(signed), cols[:, 2 * count + r : 2 * count + r + 1])
            cells = (inner + inter * across[:, :DV]) * (1.0 / divisor)
            at = slice(h * DV, (h + 1) * DV)
            gate = og_ref[rows, at].astype(F32)
            out_ref[rows, at] = (cells / (1.0 + jnp.exp(-gate)) * gain_ref[:, at]).astype(BF16)
        if c + 1 < chunks:
            kw = weighted_keys(keys, cols, 3 * count + c, heads, chunks)
            scale = pick_head(
                [decay[h * chunks + c : h * chunks + c + 1] for h in range(heads)], (width, 128), 0
            )
            rhs = jnp.concatenate([values, jnp.ones((CH, 128), BF16)], axis=1)
            state = state * jnp.concatenate([scale] * (heads + 1), axis=1) + add_outer(kw, rhs)


def mixed_cells(queries, keys, values, out_gate, in_gate, forget_gate, out_gain):
    tok_rows = queries.shape[0]
    heads = in_gate.shape[0]
    chunks = tok_rows // CH
    width = heads * DK
    ig = in_gate.reshape(heads * chunks, CH)
    fg = forget_gate.reshape(heads * chunks, CH)
    extra = -(-(1 + 2 * heads) // 8) * 8
    summary = pl.pallas_call(
        functools.partial(summary_kernel, heads, chunks),
        out_shape=jax.ShapeDtypeStruct((width + extra, 128), F32),
        in_specs=[VM] * 4,
        out_specs=VM,
        cost_estimate=pl.CostEstimate(flops=400_000_000, bytes_accessed=8_000_000, transcendentals=0),
    )(keys, values, ig, fg)
    everything = lax.all_gather(summary, "ep")
    pos = lax.axis_index("ep").astype(jnp.int32).reshape(1)
    return pl.pallas_call(
        functools.partial(cells_kernel, heads, chunks),
        out_shape=jax.ShapeDtypeStruct((tok_rows, heads * DV), BF16),
        in_specs=[pl.BlockSpec(memory_space=pltpu.SMEM)] + [VM] * 8,
        out_specs=VM,
        cost_estimate=pl.CostEstimate(flops=2_000_000_000, bytes_accessed=16_000_000, transcendentals=0),
    )(pos, queries, keys, values, out_gate, ig, fg, out_gain.reshape(1, -1), everything)


def mixer_kernel(a_ref, w_ref, out_ref):
    width = a_ref.shape[2]
    total = jnp.dot(a_ref[0], w_ref[0:width, :], preferred_element_type=F32)
    for i in range(1, a_ref.shape[0]):
        total = total + jnp.dot(
            a_ref[i], w_ref[i * width : (i + 1) * width, :], preferred_element_type=F32
        )
    out_ref[...] = total.astype(out_ref.dtype)


def mixer(gathered, weight):
    parts, rows, width = gathered.shape
    cols = weight.shape[1]
    tile = min(256, rows)
    return pl.pallas_call(
        mixer_kernel,
        grid=(rows // tile,),
        out_shape=jax.ShapeDtypeStruct((rows, cols), BF16),
        in_specs=[
            pl.BlockSpec((parts, tile, width), lambda r: (0, r, 0)),
            pl.BlockSpec((parts * width, cols), lambda r: (0, 0)),
        ],
        out_specs=pl.BlockSpec((tile, cols), lambda r: (r, 0)),
        cost_estimate=pl.CostEstimate(
            flops=2 * rows * parts * width * cols, bytes_accessed=8_000_000, transcendentals=0
        ),
    )(gathered, weight)


def hidden_kernel(x_ref, g_ref, u_ref, out_ref, gate_acc, up_acc):
    k = pl.program_id(0)
    x = x_ref[...]
    gate = jnp.dot(x, g_ref[...], preferred_element_type=F32)
    up = jnp.dot(x, u_ref[...], preferred_element_type=F32)

    @pl.when(k == 0)
    def _():
        gate_acc[...] = gate
        up_acc[...] = up

    @pl.when(k > 0)
    def _():
        gate_acc[...] += gate
        up_acc[...] += up

    @pl.when(k == pl.num_programs(0) - 1)
    def _():
        g = gate_acc[...]
        out_ref[...] = (g / (1.0 + jnp.exp(-g)) * up_acc[...]).astype(BF16)


def hidden_units(x, w_gate, w_up):
    rows, depth = x.shape
    cols = w_gate.shape[1]
    tile = min(512, depth)
    return pl.pallas_call(
        hidden_kernel,
        grid=(depth // tile,),
        out_shape=jax.ShapeDtypeStruct((rows, cols), BF16),
        in_specs=[
            pl.BlockSpec((rows, tile), lambda k: (0, k)),
            pl.BlockSpec((tile, cols), lambda k: (k, 0)),
            pl.BlockSpec((tile, cols), lambda k: (k, 0)),
        ],
        out_specs=pl.BlockSpec((rows, cols), lambda k: (0, 0)),
        scratch_shapes=[pltpu.VMEM((rows, cols), F32)] * 2,
        cost_estimate=pl.CostEstimate(
            flops=4 * rows * depth * cols,
            bytes_accessed=2 * depth * (rows + 2 * cols),
            transcendentals=0,
        ),
    )(x, w_gate, w_up)


def down_kernel(h_ref, d_ref, sh_ref, sd_ref, out_ref):
    slots = h_ref.shape[0]
    out_ref[0, 0:slots, :] = jnp.dot(h_ref[...], d_ref[...], preferred_element_type=F32).astype(BF16)
    out_ref[0, slots:, :] = jnp.dot(sh_ref[...], sd_ref[...], preferred_element_type=F32).astype(
        BF16
    )


def down_parts(hidden, w_down, shared_hidden, shared_down, blocks):
    slots, depth = hidden.shape
    shared_rows, shared_depth = shared_hidden.shape
    feat = w_down.shape[1] // blocks
    rows = slots + shared_rows
    return pl.pallas_call(
        down_kernel,
        grid=(blocks,),
        out_shape=jax.ShapeDtypeStruct((blocks, rows, feat), BF16),
        in_specs=[
            pl.BlockSpec((slots, depth), lambda j: (0, 0)),
            pl.BlockSpec((depth, feat), lambda j: (0, j)),
            pl.BlockSpec((shared_rows, shared_depth), lambda j: (0, 0)),
            pl.BlockSpec((shared_depth, feat), lambda j: (0, j)),
        ],
        out_specs=pl.BlockSpec((1, rows, feat), lambda j: (j, 0, 0)),
        cost_estimate=pl.CostEstimate(
            flops=2 * slots * depth * feat * blocks, bytes_accessed=10_000_000, transcendentals=0
        ),
    )(hidden, w_down, shared_hidden, shared_down)


def weight_columns(out_weight):
    tp_count, ep_count = lax.axis_size("tp"), lax.axis_size("ep")
    depth, features = out_weight.shape
    mine = features // tp_count
    share = mine // ep_count
    part = lax.dynamic_index_in_dim(
        out_weight.reshape(depth, tp_count, ep_count, share), lax.axis_index("ep"), 2, False
    )
    part = part.transpose(1, 0, 2)
    part = lax.all_to_all(part, "tp", split_axis=0, concat_axis=0, tiled=True)
    whole = lax.all_gather(part.reshape(tp_count * depth, share), "ep")
    return whole.transpose(1, 0, 2).reshape(tp_count * depth, mine)


def local(
    queries,
    keys,
    values,
    out_gate,
    in_gate,
    forget_gate,
    out_gain,
    out_weight,
    moe_rows,
    moe_gain,
    routes,
    route_weight,
    expert_gate,
    expert_up,
    expert_down,
    shared_gate,
    shared_up,
    shared_down,
):
    tp_count = lax.axis_size("tp")
    ep_count = lax.axis_size("ep")
    routed_rows, topk_count = routes.shape
    local_experts = expert_gate.shape[0]
    assert local_experts == 1
    expert_count = local_experts * ep_count
    capacity = 3 * routed_rows * topk_count // (2 * expert_count)
    slot_count = expert_count * capacity

    rows_wide = moe_rows.astype(F32)
    inverse = lax.rsqrt(jnp.mean(rows_wide * rows_wide, axis=1, keepdims=True) + 1e-06)
    normed = (rows_wide * inverse * moe_gain).astype(BF16)
    flat_routes = routes.reshape(-1)
    count = flat_routes.shape[0]
    onehot = flat_routes[:, None] == jnp.arange(expert_count, dtype=jnp.int32)[None, :]
    earlier = jnp.tril(jnp.ones((count, count), BF16), -1)
    before = jnp.dot(earlier, onehot.astype(BF16), preferred_element_type=F32)
    token_position = jnp.sum(jnp.where(onehot, before, 0.0), axis=1).astype(jnp.int32)
    destination = (flat_routes * capacity + token_position).reshape(routed_rows, topk_count)
    slots = jnp.arange(slot_count, dtype=jnp.int32)
    hit = destination[:, :, None] == slots[None, None, :]
    place = jnp.any(hit, axis=1).astype(BF16)
    outgoing = lax.dot_general(
        place, normed, (((0,), (0,)), ((), ())), preferred_element_type=F32
    ).astype(BF16)
    arrived = lax.all_to_all(outgoing, "ep", split_axis=0, concat_axis=0, tiled=True)

    out_columns = weight_columns(out_weight)
    mixed = mixed_cells(queries, keys, values, out_gate, in_gate, forget_gate, out_gain)
    gathered = lax.all_gather(mixed, "tp")

    shared_hidden = hidden_units(normed, shared_gate, shared_up)
    hidden = hidden_units(arrived, expert_gate[0], expert_up[0])
    parts = down_parts(hidden, expert_down[0], shared_hidden, shared_down, tp_count)
    total_rows = parts.shape[1]
    summed = lax.psum_scatter(
        parts.reshape(tp_count * total_rows, parts.shape[2]), "tp", scatter_dimension=0, tiled=True
    )
    returned = lax.all_to_all(summed[:slot_count], "ep", split_axis=0, concat_axis=0, tiled=True)
    weights = jnp.sum(jnp.where(hit, route_weight[:, :, None], 0.0), axis=1)
    picked = jnp.dot(
        weights, returned.astype(F32), precision=lax.Precision.HIGHEST, preferred_element_type=F32
    )
    moe_out = (picked + summed[slot_count:].astype(F32)).astype(BF16)
    mixer_out = mixer(gathered, out_columns)
    return (mixer_out, moe_out)


def solution(mesh):
    return jax.shard_map(
        local,
        mesh=mesh,
        in_specs=(
            P("ep", "tp"),
            P("ep", "tp"),
            P("ep", "tp"),
            P("ep", "tp"),
            P("tp", "ep"),
            P("tp", "ep"),
            P("tp"),
            P("tp", None),
            P("ep", None),
            P(),
            P("ep", None),
            P("ep", None),
            P("ep", None, "tp"),
            P("ep", None, "tp"),
            P("ep", "tp", None),
            P(None, "tp"),
            P(None, "tp"),
            P("tp", None),
        ),
        out_specs=(P("ep", "tp"), P("ep", "tp")),
        check_vma=False,
    )
```

time: 285 us -> 215 us (0.75); the launches traced: 280 us -> 213 us
  Pallas kernels: 0 us -> 42.2 us
  local copies, waits for them, and re-layouts: 51.1 us -> 12.5 us
  other arithmetic: 39.1 us -> 3.61 us
  matrix products: 39.7 us -> 4.88 us
  blocking collectives: 25 us -> 40.3 us
  waiting for transfers between devices: 100 us -> 85.2 us
    reduce_scatter x2 -> x1, waiting for transfers between devices: 75.2 us -> 2.44 us  [local(): lax.psum_scatter(parts.reshape(tp_count * total_rows, parts.shape[2]), 't...]
    all_gather x0 -> x2, waiting for transfers between devices: none -> 53.1 us  [the longest x1 46.1 us: local(): gathered = lax.all_gather(mixed, 'tp')]
    pallas_call x0 -> x6, Pallas kernels: none -> 42.2 us  [the longest x2 16.6 us: hidden_units(): pl.pallas_call(hidden_kernel, grid=(depth // tile,), out_shape=jax.ShapeD...]
    dot_general x11 -> x3, matrix products: 39.7 us -> 4.88 us  [the longest x1 2.67 us: local(): lax.dot_general(place, normed, (((0,), (0,)), ((), ())), preferred_elemen...]
    all_to_all x0 -> x1, blocking collectives: none -> 29.1 us  [weight_columns(): part = lax.all_to_all(part, 'tp', split_axis=0, concat_axis=0, tiled=True)]
    add x35 -> x2, other arithmetic: 17.5 us -> 0.71 us  [the longest x1 0.71 us: local(): flat_routes * capacity + token_position]
    unnamed x36 -> x14, local copies, waits for them, and re-layouts: 20.2 us -> 5.74 us
    convert_element_type x3 -> x2, local copies, waits for them, and re-layouts: 13.2 us -> 0.19 us  [local(): jnp.sum(jnp.where(onehot, before, 0.0), axis=1).astype(jnp.int32)]
  transfers between devices with their start and end apart: 4 -> 5, of which waited for: 3 -> 4; matrix products, arithmetic and copies ran while one was open for 34% -> 5% of each run, Pallas kernels for 0% -> 11%
where the time goes in v1:
time: 215 us; the launch traced here: 213 us
  waiting for transfers between devices  85.2 us (40%)
  Pallas kernels  42.2 us (20%)
  blocking collectives  40.3 us (19%)
  between operations  15.6 us (7%)
  local copies, waits for them, and re-layouts  12.5 us (6%)
  starting transfers between devices  8.93 us (4%)
  matrix products  4.88 us (2%)
  other arithmetic  3.61 us (2%)
    all_gather x1, waiting for transfers between devices, local(): gathered = lax.all_gather(mixed, 'tp')  46.1 us
    all_to_all x1, waiting for transfers between devices, local(): lax.all_to_all(outgoing, 'ep', split_axis=0, concat_axis=0, tiled=True)  29.6 us
    all_to_all x1, blocking collectives, weight_columns(): part = lax.all_to_all(part, 'tp', split_axis=0, concat_axis=0, tiled=True)  29.1 us
    pallas_call x2, Pallas kernels, hidden_units(): pl.pallas_call(hidden_kernel, grid=(depth // tile,), out_shape=jax.ShapeD...  16.6 us
    all_gather x1, blocking collectives, mixed_cells(): everything = lax.all_gather(summary, 'ep')  11.2 us
    pallas_call x1, Pallas kernels, down_parts(): pl.pallas_call(down_kernel, grid=(blocks,), out_shape=jax.ShapeDtypeStruc...  8.37 us
    pallas_call x1, Pallas kernels, mixed_cells(): pl.pallas_call(functools.partial(cells_kernel, heads, chunks), out_shape=...  7.17 us
    all_gather x1, waiting for transfers between devices, weight_columns(): whole = lax.all_gather(part.reshape(tp_count * depth, share), 'ep')  7.03 us
  transfers between devices with their start and end apart: 5, of which 4 were waited for; matrix products, arithmetic and copies ran while one was open for 5% of the time, Pallas kernels for 11%

profile of v1, /device:TPU:0, one launch (start us, length us, event | category | flops | bytes accessed | tf_op | source)
XLA Modules:
  0.0 213.3 jit_solution(810017691300656158)
XLA Ops:
  8.0 0.0 copy-start.2
  8.0 1.6 fusion
  9.6 0.8 copy.56
  10.4 0.1 eq.28
  10.6 0.3 fusion.4
  10.8 0.1 convert_element_type.27
  11.0 0.1 copy.57
  11.0 0.7 multiply_add_fusion
  11.8 0.1 fusion.5
  11.9 0.0 copy-done.2
  11.9 1.0 fusion.2.x_ref
  12.9 0.0 copy-start.1
  12.9 2.7 %convolution_convert_fusion = bf16[384,4096]{1,0:T(8,128)(2,1)} fusion(pred[128,384]{1,0:T(8,128)(4,1)S(1)} %fusion.5, bf16[128,4096]{1,0:T(8,128)(2,1)S(1)} %fusion.2.x_ref), kind=kOutput, calls=%fused_computation | convolution fusion | flops 404226048 | bytes 4243456 | tf_op jit(solution)/shard_map/dot_general | solution.py:398
  15.6 0.0 copy-done.1
  15.6 5.2 %all-to-all-start.1 = ((bf16[4,96,4096]{2,1,0:T(8,128)(2,1)}), bf16[4,96,4096]{2,1,0:T(8,128)(2,1)S(1)}, u32[]{:S(2)}, u32[]{:S(2)}) async-start(bf16[4,96,4096]{2,1,0:T(8,128)(2,1)} %bitcast.10), calls=%async_computation.1 | async-start | bytes 6291456 | tf_op jit(solution)/shard_map/all_to_all | solution.py:401
  20.8 0.0 reduce-scatter.2.cloned.1.call-start
  20.8 6.5 %shard_map.189.sh_ref = bf16[128,256]{1,0:T(8,128)(2,1)} custom-call(bf16[128,4096]{1,0:T(8,128)(2,1)} %copy-done.1, bf16[4096,256]{1,0:T(8,128)(2,1)} %g_ref.1, bf16[4096,256]{1,0:T(8,128)(2,1)} %u_ref.1), custom_call_target="tpu_custom_call" | custom-call | flops 536870912 | bytes 5242880 | tf_op jit(solution)/shard_map/pallas_call | solution.py:293
  27.3 29.6 %all-to-all-done.1 = bf16[4,96,4096]{2,1,0:T(8,128)(2,1)S(1)} async-done(((bf16[4,96,4096]{2,1,0:T(8,128)(2,1)}), bf16[4,96,4096]{2,1,0:T(8,128)(2,1)S(1)}, u32[]{:S(2)}, u32[]{:S(2)}) %all-to-all-start.1) | async-done | bytes 3145760 | tf_op jit(solution)/shard_map/all_to_all | solution.py:401
  56.9 1.6 copy-done
  58.6 10.1 %shard_map.188.h_ref = bf16[384,512]{1,0:T(8,128)(2,1)} custom-call(bf16[384,4096]{1,0:T(8,128)(2,1)} %bitcast.29, bf16[4096,512]{1,0:T(8,128)(2,1)} %bitcast.30, bf16[4096,512]{1,0:T(8,128)(2,1)} %bitcast.31), custom_call_target="tpu_custom_call" | custom-call | flops 3221225472 | bytes 11534336 | tf_op jit(solution)/shard_map/pallas_call | solution.py:293
  68.7 8.4 %shard_map.190 = bf16[8,512,512]{2,1,0:T(8,128)(2,1)} custom-call(bf16[384,512]{1,0:T(8,128)(2,1)} %shard_map.188.h_ref, bf16[512,4096]{1,0:T(8,128)(2,1)} %bitcast.32, bf16[128,256]{1,0:T(8,128)(2,1)} %shard_map.189.sh_ref, bf16[256,4096]{1,0:T(8,128)(2,1)} %sd_ref.1), custom_call_target="tpu_custom_call" | custom-call | flops 1610612736 | bytes 10000000 | tf_op jit(solution)/shard_map/pallas_call | solution.py:325
  77.1 0.0 reduce-scatter.2.cloned.1.call-update
  77.1 0.0 all-gather.5.cloned.1.call-start
  77.2 3.3 %copy.52 = bf16[256,4096]{0,1:T(8,128)(2,1)S(1)} copy(bf16[256,4096]{1,0:T(8,128)(2,1)} %param.25) | data formatting | bytes 4194304 | tf_op args[7]
  80.4 0.0 copy-start.3
  80.5 0.0 copy-start.4
  80.5 0.3 copy.54
  80.8 29.1 %all_to_all.28 = bf16[8,256,128]{2,1,0:T(8,128)(2,1)} all-to-all(bf16[8,256,128]{2,1,0:T(8,128)(2,1)S(1)} %copy.54), channel_id=1, replica_groups=mesh['ep'=4,'tp'=8] {'tp'}, dimensions={0} | all-to-all | bytes 1048576 | tf_op jit(solution)/shard_map/all_to_all | solution.py:351
  109.9 0.0 all-gather.5.cloned.1.call-update
  109.9 0.0 all-gather.7.cloned.1.call-start
  110.0 0.0 copy-done.3
  110.0 0.6 reshape.50.ig_ref
  110.6 0.0 copy-done.4
  110.6 0.6 reshape.51.fg_ref
  111.2 3.9 %shard_map.185 = f32[136,128]{1,0:T(8,128)} custom-call(bf16[1024,128]{1,0:T(8,128)(2,1)} %k_ref.3, bf16[1024,256]{1,0:T(8,128)(2,1)} %v_ref.3, f32[16,128]{1,0:T(8,128)} %reshape.50.ig_ref, f32[16,128]{1,0:T(8,128)} %reshape.51.fg_ref), custom_call_target="tpu_custom_call" | custom-call | flops 400000000 | bytes 8000000 | tf_op jit(solution)/shard_map/pallas_call | solution.py:220
  115.1 11.2 %all-gather = f32[544,128]{1,0:T(8,128)} all-gather(f32[136,128]{1,0:T(8,128)} %shard_map.185), channel_id=2, replica_groups=mesh['ep'=4,'tp'=8] {'ep'}, dimensions={0}, use_global_device_ids=true | all-gather | bytes 348160 | tf_op jit(solution)/shard_map/all_gather | solution.py:227
  126.3 7.2 %shard_map.186 = bf16[1024,256]{1,0:T(8,128)(2,1)} custom-call(s32[1]{0:T(128)} %bitcast.pos_ref, bf16[1024,128]{1,0:T(8,128)(2,1)} %q_ref.1, bf16[1024,128]{1,0:T(8,128)(2,1)} %k_ref.3, bf16[1024,256]{1,0:T(8,128)(2,1)} %v_ref.3, bf16[1024,256]{1,0:T(8,128)(2,1)} %og_ref.1, f32[16,128]{1,0:T(8,128)} %reshape.50.ig_ref, f32[16,128]{1,0:T(8,128)} %reshape.51.fg_ref, ...), custom_call_target="tpu_custom_call" | custom-call | flops 2000000000 | bytes 16000000 | tf_op jit(solution)/shard_map/pallas_call | solution.py:229
  133.5 0.0 all-gather.7.cloned.1.call-update
  133.5 0.1 select_reduce_fusion
  133.7 2.4 %reduce-scatter.2.cloned.1.call-done = bf16[512,512]{1,0:T(8,128)(2,1)} async-done(((bf16[4096,512]{1,0:T(8,128)(2,1)}), bf16[512,512]{1,0:T(8,128)(2,1)}) %reduce-scatter.2.cloned.1.call-update) | async-done | bytes 524304 | tf_op jit(solution)/shard_map/reduce_scatter | solution.py:411
  136.1 1.8 slice.8
  137.9 3.6 %all-to-all-start.2 = ((bf16[4,96,512]{2,1,0:T(8,128)(2,1)}), bf16[4,96,512]{2,1,0:T(8,128)(2,1)S(1)}, u32[]{:S(2)}, u32[]{:S(2)}) async-start(bf16[4,96,512]{2,1,0:T(8,128)(2,1)} %bitcast.16), calls=%async_computation.3 | async-start | bytes 786432 | tf_op jit(solution)/shard_map/all_to_all | solution.py:414
  141.5 7.0 %all-gather.5.cloned.1.call-done = bf16[4,2048,128]{2,1,0:T(8,128)(2,1)} async-done(((bf16[1,2048,128]{2,1,0:T(8,128)(2,1)}), bf16[4,2048,128]{2,1,0:T(8,128)(2,1)}) %all-gather.5.cloned.1.call-update) | async-done | bytes 2097168 | tf_op jit(solution)/shard_map/all_gather | solution.py:352
  148.5 3.1 %copy_bitcast_fusion.w_ref = bf16[2048,512]{1,0:T(8,128)(2,1)} fusion(bf16[4,2048,128]{2,1,0:T(8,128)(2,1)} %all-gather.5.cloned.1.call-done), kind=kLoop, calls=%fused_computation.6 | loop fusion | bytes 4194304 | tf_op jit(solution)/shard_map/reshape | solution.py:353
  151.7 46.1 %all-gather.7.cloned.1.call-done = bf16[8192,256]{1,0:T(8,128)(2,1)} async-done(((bf16[1024,256]{1,0:T(8,128)(2,1)}), bf16[8192,256]{1,0:T(8,128)(2,1)}) %all-gather.7.cloned.1.call-update) | async-done | bytes 4194320 | tf_op jit(solution)/shard_map/all_gather | solution.py:405
  197.8 6.2 %shard_map.187 = bf16[1024,512]{1,0:T(8,128)(2,1)} custom-call(bf16[8,1024,256]{2,1,0:T(8,128)(2,1)} %bitcast.37, bf16[2048,512]{1,0:T(8,128)(2,1)} %copy_bitcast_fusion.w_ref), custom_call_target="tpu_custom_call" | custom-call | flops 2147483648 | bytes 8000000 | tf_op jit(solution)/shard_map/pallas_call | solution.py:252
  203.9 0.0 all-to-all-done.2
  203.9 1.9 fusion.3
  (7 shorter events, 0.1 us)
Async XLA Ops:
  8.0 3.9 %copy-start.2 = (bf16[128,4096]{1,0:T(8,128)(2,1)S(1)}, bf16[128,4096]{1,0:T(8,128)(2,1)}, u32[]{:S(2)}) copy-start(bf16[128,4096]{1,0:T(8,128)(2,1)} %param.26) | copy-start | bytes 3145732
  12.9 2.7 %copy-start.1 = (bf16[128,4096]{1,0:T(8,128)(2,1)}, bf16[128,4096]{1,0:T(8,128)(2,1)S(1)}, u32[]{:S(2)}) copy-start(bf16[128,4096]{1,0:T(8,128)(2,1)S(1)} %fusion.2.x_ref) | copy-start | bytes 3145732
  15.6 41.3 %all-to-all-start.1 = ((bf16[4,96,4096]{2,1,0:T(8,128)(2,1)}), bf16[4,96,4096]{2,1,0:T(8,128)(2,1)S(1)}, u32[]{:S(2)}, u32[]{:S(2)}) async-start(bf16[4,96,4096]{2,1,0:T(8,128)(2,1)} %bitcast.10), calls=%async_computation.1 | async-start | bytes 6291456 | tf_op jit(solution)/shard_map/all_to_all | solution.py:401
  20.8 115.3 %reduce-scatter.2.cloned.1.call-start = ((), (), s32[]{:S(2)}) async-start(), calls=%async_computation.5 | async-start | bytes 4718592 | tf_op jit(solution)/shard_map/reduce_scatter | solution.py:411
  56.9 1.6 copy-start
  77.1 71.4 %all-gather.5.cloned.1.call-start = ((), (), s32[]{:S(2)}) async-start(), calls=%async_computation.4 | async-start | bytes 2621440 | tf_op jit(solution)/shard_map/all_gather | solution.py:352
  80.4 29.5 %copy-start.3 = (f32[2,1024]{1,0:T(2,128)S(1)}, f32[2,1024]{1,0:T(2,128)}, u32[]{:S(2)}) copy-start(f32[2,1024]{1,0:T(2,128)} %param.22) | copy-start | bytes 24580
  80.5 30.1 %copy-start.4 = (f32[2,1024]{1,0:T(2,128)S(1)}, f32[2,1024]{1,0:T(2,128)}, u32[]{:S(2)}) copy-start(f32[2,1024]{1,0:T(2,128)} %param.23) | copy-start | bytes 24580
  109.9 87.8 %all-gather.7.cloned.1.call-start = ((), (), s32[]{:S(2)}) async-start(), calls=%async_computation.6 | async-start | bytes 4718592 | tf_op jit(solution)/shard_map/all_gather | solution.py:405
  126.3 7.2 %copy-start.5 = (f32[128,2]{0,1:T(2,128)S(1)}, f32[128,2]{0,1:T(2,128)}, u32[]{:S(2)}) copy-start(f32[128,2]{0,1:T(2,128)} %param.29) | copy-start | bytes 3076
  137.9 66.1 %all-to-all-start.2 = ((bf16[4,96,512]{2,1,0:T(8,128)(2,1)}), bf16[4,96,512]{2,1,0:T(8,128)(2,1)S(1)}, u32[]{:S(2)}, u32[]{:S(2)}) async-start(bf16[4,96,512]{2,1,0:T(8,128)(2,1)} %bitcast.16), calls=%async_computation.3 | async-start | bytes 786432 | tf_op jit(solution)/shard_map/all_to_all | solution.py:414
Sparse Core Ops, SparseCore 0:
  77.2 58.8 reduce-scatter.1
Sparse Core Ops, SparseCore 1:
  110.0 38.5 all-gather.4
  150.6 47.1 all-gather.6

commit v2 on v1

--- a/solution.py
+++ b/solution.py
@@ -6,6 +6,7 @@
 from jax.experimental import pallas as pl
 from jax.experimental.pallas import tpu as pltpu
 from jax.sharding import PartitionSpec as P
+
 
 DK = 64
 DV = 128
@@ -118,7 +119,7 @@
     stab = [jnp.zeros((1, 128), F32) for _ in range(heads)]
     for e in range(sum_ref.shape[0]):
         reached = e < pos_ref[0]
-        part = sum_ref.at[e]
+        part = sum_ref.at[jnp.maximum(pos_ref[0] - 1 - e, 0)]
         old_w, new_w, new_stab = [], [], []
         for h in range(heads):
             at = width + 1 + h
@@ -224,7 +225,13 @@
         out_specs=VM,
         cost_estimate=pl.CostEstimate(flops=400_000_000, bytes_accessed=8_000_000, transcendentals=0),
     )(keys, values, ig, fg)
-    everything = lax.all_gather(summary, "ep")
+    ep_count = lax.axis_size("ep")
+    everything = jnp.stack(
+        [
+            lax.ppermute(summary, "ep", [(i, i + d) for i in range(ep_count - d)])
+            for d in range(1, ep_count)
+        ]
+    )
     pos = lax.axis_index("ep").astype(jnp.int32).reshape(1)
     return pl.pallas_call(
         functools.partial(cells_kernel, heads, chunks),
@@ -235,12 +242,13 @@
     )(pos, queries, keys, values, out_gate, ig, fg, out_gain.reshape(1, -1), everything)
 
 
-def mixer_kernel(a_ref, w_ref, out_ref):
-    width = a_ref.shape[2]
-    total = jnp.dot(a_ref[0], w_ref[0:width, :], preferred_element_type=F32)
-    for i in range(1, a_ref.shape[0]):
+def mixer_kernel(pos_ref, a_ref, w_ref, out_ref):
+    parts, _, width = a_ref.shape
+    total = jnp.dot(a_ref[pos_ref[0]], w_ref[0:width, :], preferred_element_type=F32)
+    for d in range(1, parts):
+        source = lax.rem(pos_ref[0] + parts - d, parts)
         total = total + jnp.dot(
-            a_ref[i], w_ref[i * width : (i + 1) * width, :], preferred_element_type=F32
+            a_ref[source], w_ref[d * width : (d + 1) * width, :], preferred_element_type=F32
         )
     out_ref[...] = total.astype(out_ref.dtype)
 
@@ -254,6 +262,7 @@
         grid=(rows // tile,),
         out_shape=jax.ShapeDtypeStruct((rows, cols), BF16),
         in_specs=[
+            pl.BlockSpec(memory_space=pltpu.SMEM),
             pl.BlockSpec((parts, tile, width), lambda r: (0, r, 0)),
             pl.BlockSpec((parts * width, cols), lambda r: (0, 0)),
         ],
@@ -261,7 +270,7 @@
         cost_estimate=pl.CostEstimate(
             flops=2 * rows * parts * width * cols, bytes_accessed=8_000_000, transcendentals=0
         ),
-    )(gathered, weight)
+    )(lax.axis_index("tp").astype(jnp.int32).reshape(1), gathered, weight)
 
 
 def hidden_kernel(x_ref, g_ref, u_ref, out_ref, gate_acc, up_acc):
@@ -344,12 +353,22 @@
     depth, features = out_weight.shape
     mine = features // tp_count
     share = mine // ep_count
-    part = lax.dynamic_index_in_dim(
-        out_weight.reshape(depth, tp_count, ep_count, share), lax.axis_index("ep"), 2, False
-    )
-    part = part.transpose(1, 0, 2)
-    part = lax.all_to_all(part, "tp", split_axis=0, concat_axis=0, tiled=True)
-    whole = lax.all_gather(part.reshape(tp_count * depth, share), "ep")
+    me, turn = lax.axis_index("tp"), lax.axis_index("ep")
+
+    def block(target):
+        return lax.dynamic_slice_in_dim(out_weight, target * mine + turn * share, share, 1)
+
+    received = [block(me)]
+    for d in range(1, tp_count):
+        received.append(
+            lax.ppermute(
+                block(lax.rem(me + d, tp_count)),
+                "tp",
+                [(i, (i + d) % tp_count) for i in range(tp_count)],
+            )
+        )
+    part = jnp.concatenate(received, axis=0)
+    whole = lax.all_gather(part, "ep")
     return whole.transpose(1, 0, 2).reshape(tp_count * depth, mine)
 
 
@@ -403,13 +422,17 @@
     out_columns = weight_columns(out_weight)
     mixed = mixed_cells(queries, keys, values, out_gate, in_gate, forget_gate, out_gain)
     gathered = lax.all_gather(mixed, "tp")
+    arrived, _ = lax.optimization_barrier((arrived, mixed))
 
     shared_hidden = hidden_units(normed, shared_gate, shared_up)
     hidden = hidden_units(arrived, expert_gate[0], expert_up[0])
     parts = down_parts(hidden, expert_down[0], shared_hidden, shared_down, tp_count)
     total_rows = parts.shape[1]
     summed = lax.psum_scatter(
-        parts.reshape(tp_count * total_rows, parts.shape[2]), "tp", scatter_dimension=0, tiled=True
+        parts.reshape(tp_count * total_rows, parts.shape[2]),
+        "tp",
+        scatter_dimension=0,
+        tiled=True,
     )
     returned = lax.all_to_all(summed[:slot_count], "ep", split_axis=0, concat_axis=0, tiled=True)
     weights = jnp.sum(jnp.where(hit, route_weight[:, :, None], 0.0), axis=1)

time: 215 us -> 212 us (0.986)
  blocking collectives: 40.3 us -> 0 us
  starting transfers between devices: 8.93 us -> 28.4 us
  waiting for transfers between devices: 85.2 us -> 103 us
    reduce_scatter x1, waiting for transfers between devices: 2.44 us -> 35.4 us  [local(): lax.psum_scatter(parts.reshape(tp_count * total_rows, parts.shape[2]), 't...]
    all_to_all x1, waiting for transfers between devices: 29.6 us -> 0.01 us  [local(): lax.all_to_all(outgoing, 'ep', split_axis=0, concat_axis=0, tiled=True)]
    all_to_all x1 -> x0, blocking collectives: 29.1 us -> none  [weight_columns(): part = lax.all_to_all(part, 'tp', split_axis=0, concat_axis=0, tiled=True)]
    ppermute x0 -> x10, waiting for transfers between devices: none -> 23.7 us  [the longest x3 16.8 us: mixed_cells(): lax.ppermute(summary, 'ep', [(i, i + d) for i in range(ep_count - d)])]
    ppermute x0 -> x10, starting transfers between devices: none -> 18.3 us  [the longest x7 9.7 us: weight_columns(): lax.ppermute(block(lax.rem(me + d, tp_count)), 'tp', [(i, (i + d) % tp_co...]
    all_gather x1 -> x0, blocking collectives: 11.2 us -> none  [mixed_cells(): everything = lax.all_gather(summary, 'ep')]
    all_gather x1, waiting for transfers between devices: 7.03 us -> 0.03 us  [weight_columns(): whole = lax.all_gather(part, 'ep')]
    all_gather x0 -> x1, local copies, waits for them, and re-layouts: none -> 3.44 us  [weight_columns(): whole = lax.all_gather(part, 'ep')]
  transfers between devices with their start and end apart: 5 -> 15, of which waited for: 4 -> 8; matrix products, arithmetic and copies ran while one was open for 5% -> 5% of each run, Pallas kernels for 11% -> 11%
where the time goes in v2:
time: 212 us; the launch traced here: 211 us
  waiting for transfers between devices  103 us (49%)
  Pallas kernels  42.2 us (20%)
  starting transfers between devices  28.4 us (13%)
  between operations  15.7 us (7%)
  local copies, waits for them, and re-layouts  12.9 us (6%)
  matrix products  4.9 us (2%)
  other arithmetic  4.31 us (2%)
    all_gather x1, waiting for transfers between devices, local(): gathered = lax.all_gather(mixed, 'tp')  43 us
    reduce_scatter x1, waiting for transfers between devices, local(): lax.psum_scatter(parts.reshape(tp_count * total_rows, parts.shape[2]), 't...  35.4 us
    ppermute x3, waiting for transfers between devices, mixed_cells(): lax.ppermute(summary, 'ep', [(i, i + d) for i in range(ep_count - d)])  16.8 us
    pallas_call x2, Pallas kernels, hidden_units(): pl.pallas_call(hidden_kernel, grid=(depth // tile,), out_shape=jax.ShapeD...  16.6 us
    ppermute x7, starting transfers between devices, weight_columns(): lax.ppermute(block(lax.rem(me + d, tp_count)), 'tp', [(i, (i + d) % tp_co...  9.7 us
    ppermute x3, starting transfers between devices, mixed_cells(): lax.ppermute(summary, 'ep', [(i, i + d) for i in range(ep_count - d)])  8.58 us
    pallas_call x1, Pallas kernels, down_parts(): pl.pallas_call(down_kernel, grid=(blocks,), out_shape=jax.ShapeDtypeStruc...  8.39 us
    pallas_call x1, Pallas kernels, mixed_cells(): pl.pallas_call(functools.partial(cells_kernel, heads, chunks), out_shape=...  7.12 us
  transfers between devices with their start and end apart: 15, of which 8 were waited for; matrix products, arithmetic and copies ran while one was open for 5% of the time, Pallas kernels for 11%

profile of v2, /device:TPU:0, one launch (start us, length us, event | category | flops | bytes accessed | tf_op | source)
XLA Modules:
  0.0 211.2 jit_solution(8332874359223497175)
XLA Ops:
  8.0 1.6 fusion
  9.6 0.8 copy.34
  10.4 0.1 eq.28
  10.6 0.3 fusion.4
  10.8 0.1 convert_element_type.27
  11.0 0.1 copy.35
  11.0 0.7 multiply_add_fusion
  11.8 0.1 fusion.5
  11.9 1.0 fusion.2.x_ref
  12.9 2.7 %convolution_convert_fusion = bf16[384,4096]{1,0:T(8,128)(2,1)} fusion(pred[128,384]{1,0:T(8,128)(4,1)S(1)} %fusion.5, bf16[128,4096]{1,0:T(8,128)(2,1)S(1)} %fusion.2.x_ref), kind=kOutput, calls=%fused_computation | convolution fusion | flops 404226048 | bytes 4243456 | tf_op jit(solution)/shard_map/dot_general | solution.py:417
  15.6 5.3 %all-to-all-start = ((bf16[4,96,4096]{2,1,0:T(8,128)(2,1)}), bf16[4,96,4096]{2,1,0:T(8,128)(2,1)S(1)}, u32[]{:S(2)}, u32[]{:S(2)}) async-start(bf16[4,96,4096]{2,1,0:T(8,128)(2,1)} %bitcast.9), calls=%async_computation | async-start | bytes 6291456 | tf_op jit(solution)/shard_map/all_to_all | solution.py:420
  21.0 0.6 reshape.51.ig_ref
  21.6 0.6 reshape.52.fg_ref
  22.2 3.9 %shard_map.185 = f32[136,128]{1,0:T(8,128)} custom-call(bf16[1024,128]{1,0:T(8,128)(2,1)} %k_ref.3, bf16[1024,256]{1,0:T(8,128)(2,1)} %v_ref.3, f32[16,128]{1,0:T(8,128)} %reshape.51.ig_ref, f32[16,128]{1,0:T(8,128)} %reshape.52.fg_ref), custom_call_target="tpu_custom_call" | custom-call | flops 400000000 | bytes 8000000 | tf_op jit(solution)/shard_map/pallas_call | solution.py:221
  26.1 3.9 %collective-permute-start = (f32[136,128]{1,0:T(8,128)}, f32[136,128]{1,0:T(8,128)S(1)}, u32[]{:S(2)}, u32[]{:S(2)}) collective-permute-start(f32[136,128]{1,0:T(8,128)} %shard_map.185), channel_id=1, source_target_pairs={{0,8},{8,16},{16,24},{1,9},{9,17},{17,25},{2,10},{10,18},{18,26},{... | collective-permute-start | bytes 208904 | tf_op jit(solution)/shard_map/ppermute | solution.py:231
  30.0 3.4 %collective-permute-start.1 = (f32[136,128]{1,0:T(8,128)}, f32[136,128]{1,0:T(8,128)S(1)}, u32[]{:S(2)}, u32[]{:S(2)}) collective-permute-start(f32[136,128]{1,0:T(8,128)} %shard_map.185), channel_id=1, source_target_pairs={{0,16},{8,24},{1,17},{9,25},{2,18},{10,26},{3,19},{11,27},{4,20},{... | collective-permute-start | bytes 208904 | tf_op jit(solution)/shard_map/ppermute | solution.py:231
  33.4 1.3 collective-permute-start.2
  34.7 6.5 %shard_map.189.sh_ref = bf16[128,256]{1,0:T(8,128)(2,1)} custom-call(bf16[128,4096]{1,0:T(8,128)(2,1)} %copy-done.1, bf16[4096,256]{1,0:T(8,128)(2,1)} %g_ref.1, bf16[4096,256]{1,0:T(8,128)(2,1)} %u_ref.1), custom_call_target="tpu_custom_call" | custom-call | flops 536870912 | bytes 5242880 | tf_op jit(solution)/shard_map/pallas_call | solution.py:302
  41.2 16.0 %collective-permute-done = f32[136,128]{1,0:T(8,128)S(1)} collective-permute-done((f32[136,128]{1,0:T(8,128)}, f32[136,128]{1,0:T(8,128)S(1)}, u32[]{:S(2)}, u32[]{:S(2)}) %collective-permute-start) | collective-permute-done | bytes 69664 | tf_op jit(solution)/shard_map/ppermute | solution.py:231
  57.2 0.7 collective-permute-done.2
  58.0 0.7 pad_maximum_fusion.sum_ref
  58.7 7.1 %shard_map.186 = bf16[1024,256]{1,0:T(8,128)(2,1)} custom-call(s32[1]{0:T(128)} %bitcast.1.pos_ref, bf16[1024,128]{1,0:T(8,128)(2,1)} %q_ref.1, bf16[1024,128]{1,0:T(8,128)(2,1)} %k_ref.3, bf16[1024,256]{1,0:T(8,128)(2,1)} %v_ref.3, bf16[1024,256]{1,0:T(8,128)(2,1)} %og_ref.1, f32[16,128]{1,0:T(8,128)} %reshape.51.ig_ref, f32[16,128]{1,0:T(8,128)} %reshape.52.fg_ref, ...), custom_call_target="tpu_custom_call" | custom-call | flops 2000000000 | bytes 16000000 | tf_op jit(solution)/shard_map/pallas_call | solution.py:236
  65.8 1.7 copy-done
  67.4 10.2 %shard_map.188.h_ref = bf16[384,512]{1,0:T(8,128)(2,1)} custom-call(bf16[384,4096]{1,0:T(8,128)(2,1)} %bitcast.26, bf16[4096,512]{1,0:T(8,128)(2,1)} %bitcast.28, bf16[4096,512]{1,0:T(8,128)(2,1)} %bitcast.29), custom_call_target="tpu_custom_call" | custom-call | flops 3221225472 | bytes 11534336 | tf_op jit(solution)/shard_map/pallas_call | solution.py:302
  77.6 8.4 %shard_map.190 = bf16[8,512,512]{2,1,0:T(8,128)(2,1)} custom-call(bf16[384,512]{1,0:T(8,128)(2,1)} %shard_map.188.h_ref, bf16[512,4096]{1,0:T(8,128)(2,1)} %bitcast.30, bf16[128,256]{1,0:T(8,128)(2,1)} %shard_map.189.sh_ref, bf16[256,4096]{1,0:T(8,128)(2,1)} %sd_ref.1), custom_call_target="tpu_custom_call" | custom-call | flops 1610612736 | bytes 10000000 | tf_op jit(solution)/shard_map/pallas_call | solution.py:334
  86.1 1.1 constant_dynamic-slice_fusion
  87.3 0.1 collective-permute-start.3
  87.3 1.9 collective-permute-start.4
  89.2 2.5 %collective-permute-start.5 = (bf16[256,128]{1,0:T(8,128)(2,1)S(1)}, bf16[256,128]{1,0:T(8,128)(2,1)S(1)}, u32[]{:S(2)}, u32[]{:S(2)}) collective-permute-start(bf16[256,128]{1,0:T(8,128)(2,1)S(1)} %get-tuple-element.7), channel_id=1, source_target_pairs={{0,3},{1,4},{2,5},{3,6},{4,7},{5,0},{6,1},{7,2},{8,11},{9,12},{10,... | collective-permute-start | bytes 196616 | tf_op jit(solution)/shard_map/ppermute | solution.py:364
  91.8 1.2 collective-permute-start.6
  93.0 1.2 collective-permute-start.7
  94.2 1.3 collective-permute-start.8
  95.6 1.5 collective-permute-start.9
  97.0 2.5 %collective-permute-done.5 = bf16[256,128]{1,0:T(8,128)(2,1)S(1)} collective-permute-done((bf16[256,128]{1,0:T(8,128)(2,1)S(1)}, bf16[256,128]{1,0:T(8,128)(2,1)S(1)}, u32[]{:S(2)}, u32[]{:S(2)}) %collective-permute-start.5) | collective-permute-done | bytes 65568 | tf_op jit(solution)/shard_map/ppermute | solution.py:364
  99.6 0.6 collective-permute-done.6
  100.2 3.2 %collective-permute-done.8 = bf16[256,128]{1,0:T(8,128)(2,1)S(1)} collective-permute-done((bf16[256,128]{1,0:T(8,128)(2,1)S(1)}, bf16[256,128]{1,0:T(8,128)(2,1)S(1)}, u32[]{:S(2)}, u32[]{:S(2)}) %collective-permute-start.8) | collective-permute-done | bytes 65568 | tf_op jit(solution)/shard_map/ppermute | solution.py:364
  103.5 0.5 collective-permute-done.9
  104.0 0.8 copy-done.3
  104.9 0.5 all-gather.5.cloned.1.call-update
  105.4 35.4 %reduce-scatter.2.cloned.1.call-done = bf16[512,512]{1,0:T(8,128)(2,1)} async-done(((bf16[4096,512]{1,0:T(8,128)(2,1)}), bf16[512,512]{1,0:T(8,128)(2,1)}) %reduce-scatter.2.cloned.1.call-update) | async-done | bytes 524304 | tf_op jit(solution)/shard_map/reduce_scatter | solution.py:431
  140.8 1.8 slice.8
  142.6 4.7 %all-to-all-start.1 = ((bf16[4,96,512]{2,1,0:T(8,128)(2,1)}), bf16[4,96,512]{2,1,0:T(8,128)(2,1)S(1)}, u32[]{:S(2)}, u32[]{:S(2)}) async-start(bf16[4,96,512]{2,1,0:T(8,128)(2,1)} %bitcast.15), calls=%async_computation.2 | async-start | bytes 786432 | tf_op jit(solution)/shard_map/all_to_all | solution.py:437
  147.3 0.1 select_reduce_fusion
  147.5 3.4 %copy.33 = bf16[4,2048,128]{2,0,1:T(4,128)(2,1)S(1)} copy(bf16[4,2048,128]{2,1,0:T(8,128)(2,1)} %bitcast.31) | data formatting | bytes 4194304 | tf_op jit(solution)/shard_map/all_gather | solution.py:371
  150.9 1.7 copy.38
  152.6 43.0 %all-gather.5.cloned.1.call-done = bf16[8192,256]{1,0:T(8,128)(2,1)} async-done(((bf16[1024,256]{1,0:T(8,128)(2,1)}), bf16[8192,256]{1,0:T(8,128)(2,1)}) %all-gather.5.cloned.1.call-update) | async-done | bytes 4194320 | tf_op jit(solution)/shard_map/all_gather | solution.py:424
  195.6 6.2 %shard_map.187 = bf16[1024,512]{1,0:T(8,128)(2,1)} custom-call(s32[1]{0:T(128)} %bitcast.pos_ref, bf16[8,1024,256]{2,1,0:T(8,128)(2,1)} %bitcast.37, bf16[2048,512]{1,0:T(8,128)(2,1)} %bitcast.32), custom_call_target="tpu_custom_call" | custom-call | flops 2147483648 | bytes 8000000 | tf_op jit(solution)/shard_map/pallas_call | solution.py:260
  201.8 1.9 fusion.3
  (34 shorter events, 0.3 us)
Async XLA Ops:
  8.0 3.9 %copy-start.2 = (bf16[128,4096]{1,0:T(8,128)(2,1)S(1)}, bf16[128,4096]{1,0:T(8,128)(2,1)}, u32[]{:S(2)}) copy-start(bf16[128,4096]{1,0:T(8,128)(2,1)} %param.26) | copy-start | bytes 3145732
  12.9 2.7 %copy-start.1 = (bf16[128,4096]{1,0:T(8,128)(2,1)}, bf16[128,4096]{1,0:T(8,128)(2,1)S(1)}, u32[]{:S(2)}) copy-start(bf16[128,4096]{1,0:T(8,128)(2,1)S(1)} %fusion.2.x_ref) | copy-start | bytes 3145732
  15.6 5.3 %copy-start.4 = (f32[2,1024]{1,0:T(2,128)S(1)}, f32[2,1024]{1,0:T(2,128)}, u32[]{:S(2)}) copy-start(f32[2,1024]{1,0:T(2,128)} %param.22) | copy-start | bytes 24580
  15.6 5.9 %copy-start.5 = (f32[2,1024]{1,0:T(2,128)S(1)}, f32[2,1024]{1,0:T(2,128)}, u32[]{:S(2)}) copy-start(f32[2,1024]{1,0:T(2,128)} %param.23) | copy-start | bytes 24580
  15.6 50.2 %all-to-all-start = ((bf16[4,96,4096]{2,1,0:T(8,128)(2,1)}), bf16[4,96,4096]{2,1,0:T(8,128)(2,1)S(1)}, u32[]{:S(2)}, u32[]{:S(2)}) async-start(bf16[4,96,4096]{2,1,0:T(8,128)(2,1)} %bitcast.9), calls=%async_computation | async-start | bytes 6291456 | tf_op jit(solution)/shard_map/all_to_all | solution.py:420
  21.0 119.9 %reduce-scatter.2.cloned.1.call-start = ((), (), s32[]{:S(2)}) async-start(), calls=%async_computation.3 | async-start | bytes 4718592 | tf_op jit(solution)/shard_map/reduce_scatter | solution.py:431
  26.1 31.1 %collective-permute-start = (f32[136,128]{1,0:T(8,128)}, f32[136,128]{1,0:T(8,128)S(1)}, u32[]{:S(2)}, u32[]{:S(2)}) collective-permute-start(f32[136,128]{1,0:T(8,128)} %shard_map.185), channel_id=1, source_target_pairs={{0,8},{8,16},{16,24},{1,9},{9,17},{17,25},{2,10},{10,18},{18,26},{... | collective-permute-start | bytes 208904 | tf_op jit(solution)/shard_map/ppermute | solution.py:231
  30.0 27.2 %collective-permute-start.1 = (f32[136,128]{1,0:T(8,128)}, f32[136,128]{1,0:T(8,128)S(1)}, u32[]{:S(2)}, u32[]{:S(2)}) collective-permute-start(f32[136,128]{1,0:T(8,128)} %shard_map.185), channel_id=1, source_target_pairs={{0,16},{8,24},{1,17},{9,25},{2,18},{10,26},{3,19},{11,27},{4,20},{... | collective-permute-start | bytes 208904 | tf_op jit(solution)/shard_map/ppermute | solution.py:231
  33.4 24.5 %collective-permute-start.2 = (f32[136,128]{1,0:T(8,128)}, f32[136,128]{1,0:T(8,128)S(1)}, u32[]{:S(2)}, u32[]{:S(2)}) collective-permute-start(f32[136,128]{1,0:T(8,128)} %shard_map.185), channel_id=1, source_target_pairs={{0,24},{1,25},{2,26},{3,27},{4,28},{5,29},{6,30},{7,31}} | collective-permute-start | bytes 208904 | tf_op jit(solution)/shard_map/ppermute | solution.py:231
  65.8 1.7 copy-start
  86.0 61.4 %all-gather.7.cloned.1.call-start = ((), (), s32[]{:S(2)}) async-start(), calls=%async_computation.5 | async-start | bytes 2621440 | tf_op jit(solution)/shard_map/all_gather | solution.py:371
  86.1 61.2 %copy-start.6 = (f32[128,2]{0,1:T(2,128)S(1)}, f32[128,2]{0,1:T(2,128)}, u32[]{:S(2)}) copy-start(f32[128,2]{0,1:T(2,128)} %param.29) | copy-start | bytes 3076
  87.3 6.9 %collective-permute-start.3 = (bf16[256,128]{1,0:T(8,128)(2,1)S(1)}, bf16[256,128]{1,0:T(8,128)(2,1)S(1)}, u32[]{:S(2)}, u32[]{:S(2)}) collective-permute-start(bf16[256,128]{1,0:T(8,128)(2,1)S(1)} %get-tuple-element.9), channel_id=1, source_target_pairs={{0,1},{1,2},{2,3},{3,4},{4,5},{5,6},{6,7},{7,0},{8,9},{9,10},{10,1... | collective-permute-start | bytes 196616 | tf_op jit(solution)/shard_map/ppermute | solution.py:364
  87.3 8.2 %collective-permute-start.4 = (bf16[256,128]{1,0:T(8,128)(2,1)S(1)}, bf16[256,128]{1,0:T(8,128)(2,1)S(1)}, u32[]{:S(2)}, u32[]{:S(2)}) collective-permute-start(bf16[256,128]{1,0:T(8,128)(2,1)S(1)} %get-tuple-element.8), channel_id=1, source_target_pairs={{0,2},{1,3},{2,4},{3,5},{4,6},{5,7},{6,0},{7,1},{8,10},{9,11},{10,... | collective-permute-start | bytes 196616 | tf_op jit(solution)/shard_map/ppermute | solution.py:364
  89.2 10.3 %collective-permute-start.5 = (bf16[256,128]{1,0:T(8,128)(2,1)S(1)}, bf16[256,128]{1,0:T(8,128)(2,1)S(1)}, u32[]{:S(2)}, u32[]{:S(2)}) collective-permute-start(bf16[256,128]{1,0:T(8,128)(2,1)S(1)} %get-tuple-element.7), channel_id=1, source_target_pairs={{0,3},{1,4},{2,5},{3,6},{4,7},{5,0},{6,1},{7,2},{8,11},{9,12},{10,... | collective-permute-start | bytes 196616 | tf_op jit(solution)/shard_map/ppermute | solution.py:364
  91.8 8.4 %collective-permute-start.6 = (bf16[256,128]{1,0:T(8,128)(2,1)S(1)}, bf16[256,128]{1,0:T(8,128)(2,1)S(1)}, u32[]{:S(2)}, u32[]{:S(2)}) collective-permute-start(bf16[256,128]{1,0:T(8,128)(2,1)S(1)} %get-tuple-element.6), channel_id=1, source_target_pairs={{0,4},{1,5},{2,6},{3,7},{4,0},{5,1},{6,2},{7,3},{8,12},{9,13},{10,... | collective-permute-start | bytes 196616 | tf_op jit(solution)/shard_map/ppermute | solution.py:364
  93.0 7.2 %collective-permute-start.7 = (bf16[256,128]{1,0:T(8,128)(2,1)S(1)}, bf16[256,128]{1,0:T(8,128)(2,1)S(1)}, u32[]{:S(2)}, u32[]{:S(2)}) collective-permute-start(bf16[256,128]{1,0:T(8,128)(2,1)S(1)} %get-tuple-element.5), channel_id=1, source_target_pairs={{0,5},{1,6},{2,7},{3,0},{4,1},{5,2},{6,3},{7,4},{8,13},{9,14},{10,... | collective-permute-start | bytes 196616 | tf_op jit(solution)/shard_map/ppermute | solution.py:364
  94.2 9.3 %collective-permute-start.8 = (bf16[256,128]{1,0:T(8,128)(2,1)S(1)}, bf16[256,128]{1,0:T(8,128)(2,1)S(1)}, u32[]{:S(2)}, u32[]{:S(2)}) collective-permute-start(bf16[256,128]{1,0:T(8,128)(2,1)S(1)} %get-tuple-element.11), channel_id=1, source_target_pairs={{0,6},{1,7},{2,0},{3,1},{4,2},{5,3},{6,4},{7,5},{8,14},{9,15},{10,... | collective-permute-start | bytes 196616 | tf_op jit(solution)/shard_map/ppermute | solution.py:364
  95.6 8.4 %collective-permute-start.9 = (bf16[256,128]{1,0:T(8,128)(2,1)S(1)}, bf16[256,128]{1,0:T(8,128)(2,1)S(1)}, u32[]{:S(2)}, u32[]{:S(2)}) collective-permute-start(bf16[256,128]{1,0:T(8,128)(2,1)S(1)} %get-tuple-element.4), channel_id=1, source_target_pairs={{0,7},{1,0},{2,1},{3,2},{4,3},{5,4},{6,5},{7,6},{8,15},{9,8},{10,9... | collective-permute-start | bytes 196616 | tf_op jit(solution)/shard_map/ppermute | solution.py:364
  104.0 0.8 copy-start.3
  104.8 90.8 %all-gather.5.cloned.1.call-start = ((), (), s32[]{:S(2)}) async-start(), calls=%async_computation.4 | async-start | bytes 4718592 | tf_op jit(solution)/shard_map/all_gather | solution.py:424
  142.6 59.2 %all-to-all-start.1 = ((bf16[4,96,512]{2,1,0:T(8,128)(2,1)}), bf16[4,96,512]{2,1,0:T(8,128)(2,1)S(1)}, u32[]{:S(2)}, u32[]{:S(2)}) async-start(bf16[4,96,512]{2,1,0:T(8,128)(2,1)} %bitcast.15), calls=%async_computation.2 | async-start | bytes 786432 | tf_op jit(solution)/shard_map/all_to_all | solution.py:437
Sparse Core Ops, SparseCore 0:
  86.1 54.6 reduce-scatter.1
Sparse Core Ops, SparseCore 1:
  104.9 41.8 all-gather.6
  148.8 46.7 all-gather.4
